TPU v7x, 32 devices: a whole 2x2x4 slice. The times are simulated.
32 devices in a mesh: gr: 2 (over x), sp: 8 (over z, y), tp: 2 (over core).
Axes of the slice: x: 2, y: 2, z: 4, core: 2. Of those that a mesh axis runs over, the one named last changes fastest.
Arguments:
- inputs: bfloat16 [4096, 2048], P(('gr', 'sp'), 'tp'), parts along dimension 0, may hold values from -6 to 6
- x_weight: bfloat16 [2048, 4096], P(None, 'tp'), may hold values from -0.125 to 0.125
- b_weight: bfloat16 [2048, 2048], P(None, 'tp'), may hold values from -0.125 to 0.125
- dt_weight: bfloat16 [2048, 128], replicated, may hold values from -0.125 to 0.125
- dt_bias: float32 [2, 64], replicated, may hold values from -2 to -1
- decay_rate: float32 [2, 64], replicated, may hold values from 0.3 to 10
- conv_x: bfloat16 [5, 4096], P(None, 'tp'), may hold values from -2.5 to 2.5
- conv_b: bfloat16 [5, 2048], P(None, 'tp'), may hold values from -2.5 to 2.5
- query_c: bfloat16 [2, 16, 128], P('gr', 'tp'), parts along dimension 0, may hold values from -6 to 6
- query_gate: bfloat16 [2, 64, 64], P('gr', 'tp'), parts along dimension 0, may hold values from -6 to 6
- read_span: int32 [2], P('gr'), parts along dimension 0, may hold values from 0 to 15
- read_gain: float32 [64, 64], P('tp'), may hold values from 0.1 to 1.9
Outputs:
- span_cache: bfloat16 [32, 2, 64, 8192], P('gr', None, 'tp', 'sp'), parts along dimension 0
- first_read: bfloat16 [2, 64, 64], P('gr', 'tp'), parts along dimension 0
There are 2 independent parts, one for each index of `gr`. A program takes and returns all parts, laid end to end along the dimension named above; an argument that names none is the same for every part. Nothing has to cross between parts.
Inputs may be any that keep to these rules, and one draw needn't show every extreme that they name: read_span holds one span index from 0 to 15.
All inputs are finite; a program needn't handle non-finite values.
Results may differ from a plain program's by a relative error of at most 0.009.
Values may be sent and summed in bfloat16 or wider, within the bound.
A program may use at most 64 MiB of HBM per device.

v0:
```python
import jax
import jax.numpy as jnp
from jax import lax
from jax.sharding import PartitionSpec as P

H = 64
P_SIZE = 64
G = 16
N = 128
KW = 5
SPAN = 128
EPSILON = 1e-06


def extended(shard, sides, width):
    for axis, dim in sides:
        size, length = (lax.axis_size(axis), shard.shape[dim])
        up = [(i, (i + 1) % size) for i in range(size - 1)]
        down = [(j, i) for i, j in up]
        last = lax.slice_in_dim(shard, length - width, length, axis=dim)
        initial = lax.slice_in_dim(shard, 0, width, axis=dim)
        before = lax.ppermute(last, axis, up)
        after = lax.ppermute(initial, axis, down)
        shard = jnp.concatenate([before, shard, after], axis=dim)
    return shard


def span_states(value_rows, key_rows, step_sizes, log_decay):
    running = jnp.cumsum(log_decay, axis=1)
    closing = running[:, -1]
    forward = jnp.exp(closing[:, None, 0] - running[:, :, 0]) * step_sizes[:, :, 0]
    backward = jnp.exp(running[:, :, 1] - log_decay[:, :, 1]) * step_sizes[:, :, 1]
    weights = jnp.stack([forward, backward], axis=2)
    states = jnp.einsum(
        "kseh,kshn,kshp->kehnp",
        weights,
        key_rows.astype(jnp.float32),
        value_rows.astype(jnp.float32),
    )
    return (states, closing)


def read_weights(span_logs, chosen):
    span_count = span_logs.shape[0]
    ahead_sum = jnp.cumsum(span_logs[:, 0], axis=0)
    behind = jnp.flip(jnp.cumsum(jnp.flip(span_logs[:, 1], 0), axis=0), 0)
    positions = jnp.arange(span_count, dtype=jnp.int32)[:, None]
    ahead_pick = lax.dynamic_slice_in_dim(ahead_sum, chosen, 1, 0)
    behind_pick = lax.dynamic_slice_in_dim(behind, chosen, 1, 0)
    before = positions <= chosen
    after = positions >= chosen
    forward = jnp.where(before, jnp.exp(jnp.where(before, ahead_pick - ahead_sum, 0.0)), 0.0)
    backward = jnp.where(after, jnp.exp(jnp.where(after, behind_pick - behind, 0.0)), 0.0)
    return jnp.stack([forward, backward], axis=1)


def per_device(
    inputs,
    x_weight,
    b_weight,
    dt_weight,
    dt_bias,
    decay_rate,
    conv_x,
    conv_b,
    query_c,
    query_gate,
    read_span,
    read_gain,
):
    tokens = inputs.shape[0]
    heads_local = x_weight.shape[1] // P_SIZE
    per_group = H // G
    tp_index = lax.axis_index("tp")
    sp_index = lax.axis_index("sp")
    dt_local = lax.dynamic_slice_in_dim(
        dt_weight.reshape(dt_weight.shape[0], 2, H), tp_index * heads_local, heads_local, 2
    )
    dt_local = dt_local.reshape(dt_weight.shape[0], 2 * heads_local)
    slab_piece = lax.all_gather(inputs, "tp", axis=1, tiled=True)
    x_part = jnp.dot(slab_piece, x_weight, preferred_element_type=jnp.float32)
    b_part = jnp.dot(slab_piece, b_weight, preferred_element_type=jnp.float32)
    dt_part = jnp.dot(slab_piece, dt_local, preferred_element_type=jnp.float32)
    joined = jnp.concatenate([x_part.astype(jnp.bfloat16), b_part.astype(jnp.bfloat16)], axis=1)
    reach = KW // 2
    padded = extended(joined, (("sp", 0),), reach)
    taps = jnp.concatenate([conv_x, conv_b], axis=1)
    mixed_rows = jnp.zeros(joined.shape, jnp.float32)
    for offset in range(KW):
        mixed_rows = mixed_rows + taps[offset].astype(jnp.float32) * padded[
            offset : offset + tokens
        ].astype(jnp.float32)
    mixed_rows = jax.nn.silu(mixed_rows).astype(jnp.bfloat16)
    split_at = x_weight.shape[1]
    values = mixed_rows[:, :split_at]
    key_rows = mixed_rows[:, split_at:]
    length = tokens * lax.axis_size("sp")
    bias_local = lax.dynamic_slice_in_dim(dt_bias, tp_index * heads_local, heads_local, 1)
    rate_local = lax.dynamic_slice_in_dim(decay_rate, tp_index * heads_local, heads_local, 1)
    dt_raw = dt_part.astype(jnp.bfloat16).reshape(tokens, 2, heads_local)
    step_sizes = jax.nn.softplus(dt_raw.astype(jnp.float32) + bias_local)
    log_decay = -(step_sizes * rate_local) / length
    span_count = tokens // SPAN
    value_rows = values.reshape(span_count, SPAN, heads_local, P_SIZE)
    group_keys = key_rows.reshape(span_count, SPAN, heads_local // per_group, N)
    group_keys = jnp.repeat(group_keys, per_group, axis=2)
    states, closing = span_states(
        value_rows,
        group_keys,
        step_sizes.reshape(span_count, SPAN, 2, heads_local),
        log_decay.reshape(span_count, SPAN, 2, heads_local),
    )
    local_rows = states.reshape(span_count, 2, heads_local, N * P_SIZE).astype(jnp.bfloat16)
    all_logs = lax.all_gather(closing, "sp", axis=0, tiled=True)
    weights = read_weights(all_logs, read_span[0])
    cache_rows = lax.all_to_all(local_rows, "sp", split_axis=3, concat_axis=0, tiled=True)
    columns = cache_rows.shape[3] // P_SIZE
    gathered = jnp.einsum("jeh,jehx->hx", weights, cache_rows.astype(jnp.float32)).reshape(
        heads_local, columns, P_SIZE
    )
    picked = lax.dynamic_slice_in_dim(query_c[0], sp_index * columns, columns, 1)
    query_cols = jnp.repeat(picked.astype(jnp.float32), per_group, axis=0)
    partial_read = jnp.einsum("hnp,hn->hp", gathered, query_cols)
    read_total = lax.psum(partial_read, "sp")
    gated_read = read_total * jax.nn.silu(query_gate[0].astype(jnp.float32))
    square_sum = lax.psum(jnp.sum(gated_read * gated_read), "tp")
    mean_square = square_sum / (H * P_SIZE)
    first_read = (gated_read * lax.rsqrt(mean_square + EPSILON) * read_gain)[None].astype(
        jnp.bfloat16
    )
    return (cache_rows, first_read)


def solution(mesh):
    return jax.shard_map(
        per_device,
        mesh=mesh,
        in_specs=(
            P(("gr", "sp"), "tp"),
            P(None, "tp"),
            P(None, "tp"),
            P(),
            P(),
            P(),
            P(None, "tp"),
            P(None, "tp"),
            P("gr", "tp", None),
            P("gr", "tp", None),
            P("gr"),
            P("tp", None),
        ),
        out_specs=(P("gr", None, "tp", "sp"), P("gr", "tp", None)),
        check_vma=False,
    )
```

profile of v0, /device:TPU:0, one launch (start us, length us, event | category | flops | bytes accessed | tf_op | source)
XLA Modules:
  0.0 222.9 jit_solution(17773302501208012883)
XLA Ops:
  7.2 0.7 all-gather.3.cloned.1.call-update
  7.9 0.8 constant_dynamic-update-slice_fusion.1
  8.7 0.8 constant_dynamic-slice_fusion.2
  9.4 1.2 copy.63
  10.7 0.7 constant_dynamic-update-slice_fusion
  11.5 9.8 %all-gather.3.cloned.1.call-done = bf16[256,2048]{1,0:T(8,128)(2,1)} async-done(((bf16[256,1024]{1,0:T(8,128)(2,1)}), bf16[256,2048]{1,0:T(8,128)(2,1)}) %all-gather.3.cloned.1.call-update) | async-done | bytes 1048592 | tf_op jit(solution)/shard_map/all_gather | solution.py:80
  21.3 1.8 fusion.9
  23.2 0.2 copy.65
  23.5 0.2 fusion.24
  23.9 5.9 %convolution_convert_fusion = bf16[256,2048]{1,0:T(8,128)(2,1)S(1)} fusion(bf16[256,2048]{1,0:T(8,128)(2,1)S(1)} %copy-done.1, bf16[2048,2048]{1,0:T(8,128)(2,1)} %param.13), kind=kOutput, calls=%fused_computation.3 | convolution fusion | flops 2148007936 | bytes 10485760 | tf_op jit(solution)/shard_map/dot_general | solution.py:81
  29.8 1.3 convolution_convert_fusion.1
  31.1 3.6 %collective-permute-start = (bf16[2,3072]{1,0:T(2,128)(2,1)S(1)}, bf16[2,3072]{1,0:T(2,128)(2,1)S(1)}, u32[]{:S(2)}, u32[]{:S(2)}) collective-permute-start(bf16[2,3072]{1,0:T(2,128)(2,1)S(1)} %get-tuple-element.6), channel_id=1, source_target_pairs={{0,2},{2,4},{4,6},{6,8},{8,10},{10,12},{12,14},{1,3},{3,5},{5,7},{... | collective-permute-start | bytes 36872 | tf_op jit(solution)/shard_map/ppermute | solution.py:22
  34.8 1.3 collective-permute-start.1
  36.3 4.1 %collective-permute-done.1 = bf16[2,3072]{1,0:T(2,128)(2,1)S(1)} collective-permute-done((bf16[2,3072]{1,0:T(2,128)(2,1)S(1)}, bf16[2,3072]{1,0:T(2,128)(2,1)S(1)}, u32[]{:S(2)}, u32[]{:S(2)}) %collective-permute-start.1) | collective-permute-done | bytes 12320 | tf_op jit(solution)/shard_map/ppermute | solution.py:23
  40.4 0.5 maximum_maximum_fusion
  40.9 2.9 %multiply_convert_fusion = bf16[256,3072]{1,0:T(8,128)(2,1)S(1)} fusion(bf16[256,1024]{1,0:T(8,128)(2,1)S(1)} %convolution_convert_fusion.1, bf16[256,2048]{1,0:T(8,128)(2,1)S(1)} %convolution_convert_fusion, bf16[258,3072]{1,0:T(8,128)(2,1)S(1)} %get-tuple-element.5, bf16[258,3072]{1,0:T(8,128)(2,1)S(1)} %get-tuple-element.4, f32[3072]{0:T(1024)S(1)} %bitcast.103, ...), kind=kLoop, calls=%fused_computation.2 | loop fusion | flops 17301504 | bytes 9498624 | tf_op jit(solution)/shard_map/convert_element_type | solution.py:93
  43.7 0.2 slice_convert_fusion
  44.0 3.0 %reshape.152 = f32[2,128,32,64]{3,2,1,0:T(8,128)} reshape(f32[256,2048]{1,0:T(8,128)S(1)} %slice_convert_fusion) | data formatting | bytes 4194304 | tf_op jit(solution)/shard_map/convert.7
  47.0 3.8 %copy.62 = f32[2,128,32,64]{1,3,2,0:T(8,128)S(1)} copy(f32[2,128,32,64]{3,2,1,0:T(8,128)} %reshape.152) | data formatting | bytes 4194304 | tf_op jit(solution)/shard_map/convert.7
  51.0 0.6 broadcast_in_dim.43
  51.6 2.0 convert_bitcast_fusion
  53.6 14.1 %copy.82 = bf16[2,2,32,128,64]{2,1,0,4,3:T(2,128)(2,1)} copy(bf16[2,2,32,128,64]{3,4,1,2,0:T(8,128)(2,1)} %convert_bitcast_fusion) | data formatting | bytes 4194304 | tf_op jit(solution)/shard_map/convert_element_type | solution.py:113
  67.7 11.2 %reshape.153 = bf16[8,2,65536]{2,1,0:T(2,128)(2,1)} reshape(bf16[8192,2,2,32]{3,2,1,0:T(2,128)(2,1)} %bitcast.92) | data formatting | bytes 4194304
  78.9 5.6 %all-to-all-start = ((bf16[8,2,65536]{2,1,0:T(2,128)(2,1)}), bf16[8,2,65536]{2,1,0:T(2,128)(2,1)S(1)}, u32[]{:S(2)}, u32[]{:S(2)}) async-start(bf16[8,2,65536]{2,1,0:T(2,128)(2,1)} %reshape.153), calls=%async_computation | async-start | bytes 4194304 | tf_op jit(solution)/shard_map/all_to_all | solution.py:116
  85.2 65.2 %all-gather = f32[16,1,2,32]{3,2,1,0:T(2,128)S(1)} all-gather(f32[2,1,2,32]{3,2,1,0:T(2,128)S(1)} %get-tuple-element.8), channel_id=2, replica_groups=mesh['gr'=2,'sp'=8,'tp'=2] {'sp'}, dimensions={0}, use_global_device_ids=true | all-gather | bytes 4608 | tf_op jit(solution)/shard_map/all_gather | solution.py:114
  150.8 6.6 %reshape.154 = bf16[8192,2,2,32]{3,2,1,0:T(2,128)(2,1)} reshape(bf16[8,2,65536]{2,1,0:T(2,128)(2,1)S(1)} %all-to-all-done) | data formatting | bytes 4194304
  157.4 17.8 %copy.84 = bf16[2,2,32,8,1024]{4,2,1,0,3:T(8,128)(2,1)S(1)} copy(bf16[2,2,32,8,1024]{2,1,0,4,3:T(2,128)(2,1)} %bitcast.93) | data formatting | bytes 4194304 | tf_op jit(solution)/shard_map/all_to_all | solution.py:116
  175.2 2.4 %fusion.2 = bf16[32,1,1024,1]{2,1,3,0:T(2,128)(2,1)S(1)} fusion(bf16[16,2,32,1]{0,3,1,2:T(2,128)(2,1)S(1)} %copy.75, bf16[16,2,32,1024]{3,2,1,0:T(8,128)(2,1)S(1)} %bitcast.95), kind=kOutput, calls=%fused_computation.7 | convolution fusion | flops 2097152 | bytes 2164736 | tf_op jit(solution)/shard_map/jeh,jehx->hx/dot_general | solution.py:118
  178.0 33.1 %psum.14 = f32[32,64]{1,0:T(8,128)S(1)} all-reduce(f32[32,64]{1,0:T(8,128)S(1)} %bitcast.110), channel_id=1, replica_groups=mesh['gr'=2,'sp'=8,'tp'=2] {'sp'}, use_global_device_ids=true, to_apply=%region_3.4 | all-reduce | flops 2048 | bytes 16384 | tf_op jit(solution)/shard_map/psum | solution.py:124
  211.0 0.6 multiply_reduce_fusion
  211.7 3.1 %psum.15 = f32[]{:T(128)} all-reduce(f32[]{:T(128)} %multiply_reduce_fusion), channel_id=1, replica_groups=mesh['gr'=2,'sp'=8,'tp'=2] {'tp'}, use_global_device_ids=true, to_apply=%region_5.6 | all-reduce | flops 1 | bytes 8 | tf_op jit(solution)/shard_map/psum | solution.py:126
  215.4 0.6 fusion.17
  (48 shorter events, 1.8 us)
Async XLA Ops:
  7.2 14.1 %all-gather.3.cloned.1.call-start = ((), (), s32[]{:S(2)}) async-start(), calls=%async_computation.1 | async-start | bytes 1572864 | tf_op jit(solution)/shard_map/all_gather | solution.py:80
  21.3 2.6 %copy-start.1 = (bf16[256,2048]{1,0:T(8,128)(2,1)S(1)}, bf16[256,2048]{1,0:T(8,128)(2,1)}, u32[]{:S(2)}) copy-start(bf16[256,2048]{1,0:T(8,128)(2,1)} %all-gather.3.cloned.1.call-done) | copy-start | bytes 3145732
  23.9 5.9 %copy-start.5 = (bf16[2048,1024]{1,0:T(8,128)(2,1)S(1)}, bf16[2048,1024]{1,0:T(8,128)(2,1)}, u32[]{:S(2)}) copy-start(bf16[2048,1024]{1,0:T(8,128)(2,1)} %param.14) | copy-start | bytes 12582916
  31.1 5.1 %collective-permute-start = (bf16[2,3072]{1,0:T(2,128)(2,1)S(1)}, bf16[2,3072]{1,0:T(2,128)(2,1)S(1)}, u32[]{:S(2)}, u32[]{:S(2)}) collective-permute-start(bf16[2,3072]{1,0:T(2,128)(2,1)S(1)} %get-tuple-element.6), channel_id=1, source_target_pairs={{0,2},{2,4},{4,6},{6,8},{8,10},{10,12},{12,14},{1,3},{3,5},{5,7},{... | collective-permute-start | bytes 36872 | tf_op jit(solution)/shard_map/ppermute | solution.py:22
  34.8 5.6 %collective-permute-start.1 = (bf16[2,3072]{1,0:T(2,128)(2,1)S(1)}, bf16[2,3072]{1,0:T(2,128)(2,1)S(1)}, u32[]{:S(2)}, u32[]{:S(2)}) collective-permute-start(bf16[2,3072]{1,0:T(2,128)(2,1)S(1)} %get-tuple-element.7), channel_id=1, source_target_pairs={{2,0},{4,2},{6,4},{8,6},{10,8},{12,10},{14,12},{3,1},{5,3},{7,5},{... | collective-permute-start | bytes 36872 | tf_op jit(solution)/shard_map/ppermute | solution.py:23
  78.8 6.3 %copy-start.4 = (bf16[1,8,128]{2,1,0:T(8,128)(2,1)S(1)}, bf16[1,8,128]{2,1,0:T(8,128)(2,1)}, u32[]{:S(2)}) copy-start(bf16[1,8,128]{2,1,0:T(8,128)(2,1)} %param.20) | copy-start | bytes 6148
  78.9 72.0 %all-to-all-start = ((bf16[8,2,65536]{2,1,0:T(2,128)(2,1)}), bf16[8,2,65536]{2,1,0:T(2,128)(2,1)S(1)}, u32[]{:S(2)}, u32[]{:S(2)}) async-start(bf16[8,2,65536]{2,1,0:T(2,128)(2,1)} %reshape.153), calls=%async_computation | async-start | bytes 4194304 | tf_op jit(solution)/shard_map/all_to_all | solution.py:116
  157.4 53.7 %copy-start.2 = (bf16[1,32,64]{2,1,0:T(8,128)(2,1)S(1)}, bf16[1,32,64]{2,1,0:T(8,128)(2,1)}, u32[]{:S(2)}) copy-start(bf16[1,32,64]{2,1,0:T(8,128)(2,1)} %param.21) | copy-start | bytes 12292
  175.2 40.9 %copy-start = (bf16[2,2,32,8,1024]{4,2,1,0,3:T(8,128)(2,1)}, bf16[2,2,32,8,1024]{4,2,1,0,3:T(8,128)(2,1)S(1)}, u32[]{:S(2)}) copy-start(bf16[2,2,32,8,1024]{4,2,1,0,3:T(8,128)(2,1)S(1)} %copy.84) | copy-start | bytes 6291460
  175.2 40.2 %copy-start.3 = (f32[32,64]{1,0:T(8,128)S(1)}, f32[32,64]{1,0:T(8,128)}, u32[]{:S(2)}) copy-start(f32[32,64]{1,0:T(8,128)} %param.23) | copy-start | bytes 24580
Sparse Core Ops, SparseCore 0:
  9.5 11.7 all-gather.2
where the time goes:
time: 224 us; the launch traced here: 223 us
  blocking collectives  101 us (45%)
  local copies, waits for them, and re-layouts  61.6 us (28%)
  between operations  15.7 us (7%)
  waiting for transfers between devices  14.6 us (7%)
  matrix products  13.5 us (6%)
  starting transfers between devices  10.6 us (5%)
  other arithmetic  5.54 us (2%)
    all_gather x1, blocking collectives, per_device(): all_logs = lax.all_gather(closing, 'sp', axis=0, tiled=True)  65.2 us
    psum x1, blocking collectives, per_device(): read_total = lax.psum(partial_read, 'sp')  33.1 us
    unnamed x20, local copies, waits for them, and re-layouts  20.1 us
    all_to_all x1, local copies, waits for them, and re-layouts, per_device(): lax.all_to_all(local_rows, 'sp', split_axis=3, concat_axis=0, tiled=True)  17.8 us
    convert_element_type x1, local copies, waits for them, and re-layouts, per_device(): states.reshape(span_count, 2, heads_local, N * P_SIZE).astype(jnp.bfloat16)  14.1 us
    all_gather x1, waiting for transfers between devices, per_device(): slab_piece = lax.all_gather(inputs, 'tp', axis=1, tiled=True)  9.82 us
    another operation x2, local copies, waits for them, and re-layouts  6.77 us
    dot_general x1, matrix products, per_device(): x_part = jnp.dot(slab_piece, x_weight, preferred_element_type=jnp.float32)  5.86 us
  transfers between devices with their start and end apart: 4, of which 2 were waited for; matrix products, arithmetic and copies ran while one was open for 2% of the time, Pallas kernels for 0%

commit v1 on v0

--- a/solution.py
+++ b/solution.py
@@ -113,7 +113,10 @@
     local_rows = states.reshape(span_count, 2, heads_local, N * P_SIZE).astype(jnp.bfloat16)
     all_logs = lax.all_gather(closing, "sp", axis=0, tiled=True)
     weights = read_weights(all_logs, read_span[0])
-    cache_rows = lax.all_to_all(local_rows, "sp", split_axis=3, concat_axis=0, tiled=True)
+    cache_rows = jnp.concatenate(
+        lax.all_to_all(jnp.stack(jnp.split(local_rows, lax.axis_size("sp"), axis=3)), "sp", 0, 0),
+        axis=0,
+    )
     columns = cache_rows.shape[3] // P_SIZE
     gathered = jnp.einsum("jeh,jehx->hx", weights, cache_rows.astype(jnp.float32)).reshape(
         heads_local, columns, P_SIZE

time: 224 us -> 192 us (0.86)
  local copies, waits for them, and re-layouts: 61.6 us -> 29.5 us
    all_to_all x1 -> x0, local copies, waits for them, and re-layouts: 17.8 us -> none  [per_device(): lax.all_to_all(local_rows, 'sp', split_axis=3, concat_axis=0, tiled=True)]
    unnamed x20 -> x24, local copies, waits for them, and re-layouts: 20.1 us -> 8.68 us
    convert_element_type x1 -> x2, local copies, waits for them, and re-layouts: 14.1 us -> 10.4 us  [per_device(): states.reshape(span_count, 2, heads_local, N * P_SIZE).astype(jnp.bfloat16)]
    another operation x2 -> x3, local copies, waits for them, and re-layouts: 6.77 us -> 7.5 us
where the time goes in v1:
time: 192 us; the launch traced here: 191 us
  blocking collectives  101 us (53%)
  local copies, waits for them, and re-layouts  29.5 us (15%)
  between operations  15.7 us (8%)
  waiting for transfers between devices  14.6 us (8%)
  matrix products  13.5 us (7%)
  starting transfers between devices  10.6 us (6%)
  other arithmetic  5.54 us (3%)
    all_gather x1, blocking collectives, per_device(): all_logs = lax.all_gather(closing, 'sp', axis=0, tiled=True)  65.1 us
    psum x1, blocking collectives, per_device(): read_total = lax.psum(partial_read, 'sp')  33.1 us
    convert_element_type x2, local copies, waits for them, and re-layouts, per_device(): states.reshape(span_count, 2, heads_local, N * P_SIZE).astype(jnp.bfloat16)  10.4 us
    all_gather x1, waiting for transfers between devices, per_device(): slab_piece = lax.all_gather(inputs, 'tp', axis=1, tiled=True)  9.82 us
    unnamed x24, local copies, waits for them, and re-layouts  8.68 us
    another operation x2, local copies, waits for them, and re-layouts  6.78 us
    dot_general x1, matrix products, per_device(): x_part = jnp.dot(slab_piece, x_weight, preferred_element_type=jnp.float32)  5.86 us
    all_to_all x1, starting transfers between devices, per_device(): lax.all_to_all(jnp.stack(jnp.split(local_rows, lax.axis_size('sp'), axis=...  5.63 us
  transfers between devices with their start and end apart: 4, of which 2 were waited for; matrix products, arithmetic and copies ran while one was open for 2% of the time, Pallas kernels for 0%

profile of v1, /device:TPU:0, one launch (start us, length us, event | category | flops | bytes accessed | tf_op | source)
XLA Modules:
  0.0 190.8 jit_solution(12353510731553552230)
XLA Ops:
  7.2 0.7 all-gather.3.cloned.1.call-update
  7.9 0.8 constant_dynamic-update-slice_fusion.1
  8.7 0.8 constant_dynamic-slice_fusion.2
  9.4 1.2 copy.49
  10.7 0.7 constant_dynamic-update-slice_fusion
  11.5 9.8 %all-gather.3.cloned.1.call-done = bf16[256,2048]{1,0:T(8,128)(2,1)} async-done(((bf16[256,1024]{1,0:T(8,128)(2,1)}), bf16[256,2048]{1,0:T(8,128)(2,1)}) %all-gather.3.cloned.1.call-update) | async-done | bytes 1048592 | tf_op jit(solution)/shard_map/all_gather | solution.py:80
  21.3 1.8 fusion.9
  23.9 5.9 %convolution_convert_fusion = bf16[256,2048]{1,0:T(8,128)(2,1)S(1)} fusion(bf16[256,2048]{1,0:T(8,128)(2,1)S(1)} %copy-done, bf16[2048,2048]{1,0:T(8,128)(2,1)} %param.13), kind=kOutput, calls=%fused_computation.3 | convolution fusion | flops 2148007936 | bytes 10485760 | tf_op jit(solution)/shard_map/dot_general | solution.py:81
  29.8 1.3 convolution_convert_fusion.1
  31.1 3.6 %collective-permute-start = (bf16[2,3072]{1,0:T(2,128)(2,1)S(1)}, bf16[2,3072]{1,0:T(2,128)(2,1)S(1)}, u32[]{:S(2)}, u32[]{:S(2)}) collective-permute-start(bf16[2,3072]{1,0:T(2,128)(2,1)S(1)} %get-tuple-element.6), channel_id=1, source_target_pairs={{0,2},{2,4},{4,6},{6,8},{8,10},{10,12},{12,14},{1,3},{3,5},{5,7},{... | collective-permute-start | bytes 36872 | tf_op jit(solution)/shard_map/ppermute | solution.py:22
  34.8 1.3 collective-permute-start.1
  36.3 4.1 %collective-permute-done.1 = bf16[2,3072]{1,0:T(2,128)(2,1)S(1)} collective-permute-done((bf16[2,3072]{1,0:T(2,128)(2,1)S(1)}, bf16[2,3072]{1,0:T(2,128)(2,1)S(1)}, u32[]{:S(2)}, u32[]{:S(2)}) %collective-permute-start.1) | collective-permute-done | bytes 12320 | tf_op jit(solution)/shard_map/ppermute | solution.py:23
  40.9 2.9 %multiply_convert_fusion = bf16[256,3072]{1,0:T(8,128)(2,1)S(1)} fusion(bf16[256,1024]{1,0:T(8,128)(2,1)S(1)} %convolution_convert_fusion.1, bf16[256,2048]{1,0:T(8,128)(2,1)S(1)} %convolution_convert_fusion, bf16[258,3072]{1,0:T(8,128)(2,1)S(1)} %get-tuple-element.5, bf16[258,3072]{1,0:T(8,128)(2,1)S(1)} %get-tuple-element.4, f32[3072]{0:T(1024)S(1)} %bitcast.128, ...), kind=kLoop, calls=%fused_computation.2 | loop fusion | flops 17301504 | bytes 9498624 | tf_op jit(solution)/shard_map/convert_element_type | solution.py:93
  44.0 3.0 %reshape.156 = f32[2,128,32,64]{3,2,1,0:T(8,128)} reshape(f32[256,2048]{1,0:T(8,128)S(1)} %slice_convert_fusion) | data formatting | bytes 4194304 | tf_op jit(solution)/shard_map/convert.7
  47.0 3.8 %copy.48 = f32[2,128,32,64]{1,3,2,0:T(8,128)S(1)} copy(f32[2,128,32,64]{3,2,1,0:T(8,128)} %reshape.156) | data formatting | bytes 4194304 | tf_op jit(solution)/shard_map/convert.7
  51.6 2.0 %convert_bitcast_fusion = bf16[2,2,32,128,64]{3,4,1,2,0:T(8,128)(2,1)} fusion(bf16[2,128,32,128,1]{3,1,4,2,0:T(8,128)(2,1)S(1)} %bitcast.119, f32[2,128,32,2]{1,3,2,0:T(2,128)S(1)} %copy.54, f32[2,128,32,64]{1,3,2,0:T(8,128)S(1)} %copy.48), kind=kOutput, calls=%fused_computation.9 | convolution fusion | flops 270532608 | bytes 6356992 | tf_op jit(solution)/shard_map/kseh,kshn,kshp->kehnp/dot_general | solution.py:34
  53.6 4.8 %copy.56 = bf16[2,2,32,128,64]{4,3,2,1,0:T(8,128)(2,1)} copy(bf16[2,2,32,128,64]{3,4,1,2,0:T(8,128)(2,1)} %convert_bitcast_fusion) | data formatting | bytes 4194304 | tf_op jit(solution)/shard_map/convert_element_type | solution.py:113
  58.4 5.7 %convert_element_type.93 = bf16[2,2,32,8192]{3,2,1,0:T(8,128)(2,1)S(1)} reshape(bf16[2,2,32,128,64]{4,3,2,1,0:T(8,128)(2,1)} %copy.56) | data formatting | bytes 4194304 | tf_op jit(solution)/shard_map/convert_element_type | solution.py:113
  64.0 0.7 fusion.17
  64.8 0.7 fusion.16
  65.5 0.7 fusion.15
  66.2 0.7 fusion.14
  66.9 0.7 fusion.13
  67.6 0.7 fusion.12
  68.4 0.7 fusion.11
  69.1 0.7 fusion.10
  69.8 5.6 %all-to-all-start = ((bf16[8,2,2,32,1024]{4,3,2,1,0:T(8,128)(2,1)}), bf16[8,2,2,32,1024]{4,3,2,1,0:T(8,128)(2,1)S(1)}, u32[]{:S(2)}, u32[]{:S(2)}) async-start(bf16[8,2,2,32,1024]{4,3,2,1,0:T(8,128)(2,1)} %fusion.10), calls=%async_computation | async-start | bytes 4194304 | tf_op jit(solution)/shard_map/all_to_all | solution.py:117
  76.2 65.1 %all-gather = f32[16,1,2,32]{3,2,1,0:T(2,128)S(1)} all-gather(f32[2,1,2,32]{3,2,1,0:T(2,128)S(1)} %get-tuple-element.8), channel_id=2, replica_groups=mesh['gr'=2,'sp'=8,'tp'=2] {'sp'}, dimensions={0}, use_global_device_ids=true | all-gather | bytes 4608 | tf_op jit(solution)/shard_map/all_gather | solution.py:114
  141.8 2.4 %fusion.2 = bf16[32,1,1024,1]{2,1,3,0:T(2,128)(2,1)S(1)} fusion(bf16[16,2,32,1]{0,3,1,2:T(2,128)(2,1)S(1)} %copy.58, bf16[16,2,32,1024]{3,2,1,0:T(8,128)(2,1)S(1)} %bitcast.120), kind=kOutput, calls=%fused_computation.7 | convolution fusion | flops 2097152 | bytes 2164736 | tf_op jit(solution)/shard_map/jeh,jehx->hx/dot_general | solution.py:121
  144.5 33.1 %psum.14 = f32[32,64]{1,0:T(8,128)S(1)} all-reduce(f32[32,64]{1,0:T(8,128)S(1)} %bitcast.135), channel_id=1, replica_groups=mesh['gr'=2,'sp'=8,'tp'=2] {'sp'}, use_global_device_ids=true, to_apply=%region_3.4 | all-reduce | flops 2048 | bytes 16384 | tf_op jit(solution)/shard_map/psum | solution.py:127
  178.2 3.1 %psum.15 = f32[]{:T(128)} all-reduce(f32[]{:T(128)} %multiply_reduce_fusion), channel_id=1, replica_groups=mesh['gr'=2,'sp'=8,'tp'=2] {'tp'}, use_global_device_ids=true, to_apply=%region_5.6 | all-reduce | flops 1 | bytes 8 | tf_op jit(solution)/shard_map/psum | solution.py:129
  182.6 1.3 copy.86
  (53 shorter events, 4.6 us)
Async XLA Ops:
  7.2 14.1 %all-gather.3.cloned.1.call-start = ((), (), s32[]{:S(2)}) async-start(), calls=%async_computation.1 | async-start | bytes 1572864 | tf_op jit(solution)/shard_map/all_gather | solution.py:80
  21.3 2.6 %copy-start = (bf16[256,2048]{1,0:T(8,128)(2,1)S(1)}, bf16[256,2048]{1,0:T(8,128)(2,1)}, u32[]{:S(2)}) copy-start(bf16[256,2048]{1,0:T(8,128)(2,1)} %all-gather.3.cloned.1.call-done) | copy-start | bytes 3145732
  23.9 5.9 %copy-start.4 = (bf16[2048,1024]{1,0:T(8,128)(2,1)S(1)}, bf16[2048,1024]{1,0:T(8,128)(2,1)}, u32[]{:S(2)}) copy-start(bf16[2048,1024]{1,0:T(8,128)(2,1)} %param.14) | copy-start | bytes 12582916
  31.1 5.1 %collective-permute-start = (bf16[2,3072]{1,0:T(2,128)(2,1)S(1)}, bf16[2,3072]{1,0:T(2,128)(2,1)S(1)}, u32[]{:S(2)}, u32[]{:S(2)}) collective-permute-start(bf16[2,3072]{1,0:T(2,128)(2,1)S(1)} %get-tuple-element.6), channel_id=1, source_target_pairs={{0,2},{2,4},{4,6},{6,8},{8,10},{10,12},{12,14},{1,3},{3,5},{5,7},{... | collective-permute-start | bytes 36872 | tf_op jit(solution)/shard_map/ppermute | solution.py:22
  34.8 5.6 %collective-permute-start.1 = (bf16[2,3072]{1,0:T(2,128)(2,1)S(1)}, bf16[2,3072]{1,0:T(2,128)(2,1)S(1)}, u32[]{:S(2)}, u32[]{:S(2)}) collective-permute-start(bf16[2,3072]{1,0:T(2,128)(2,1)S(1)} %get-tuple-element.7), channel_id=1, source_target_pairs={{2,0},{4,2},{6,4},{8,6},{10,8},{12,10},{14,12},{3,1},{5,3},{7,5},{... | collective-permute-start | bytes 36872 | tf_op jit(solution)/shard_map/ppermute | solution.py:23
  69.8 6.3 %copy-start.3 = (bf16[1,8,128]{2,1,0:T(8,128)(2,1)S(1)}, bf16[1,8,128]{2,1,0:T(8,128)(2,1)}, u32[]{:S(2)}) copy-start(bf16[1,8,128]{2,1,0:T(8,128)(2,1)} %param.20) | copy-start | bytes 6148
  69.8 72.0 %all-to-all-start = ((bf16[8,2,2,32,1024]{4,3,2,1,0:T(8,128)(2,1)}), bf16[8,2,2,32,1024]{4,3,2,1,0:T(8,128)(2,1)S(1)}, u32[]{:S(2)}, u32[]{:S(2)}) async-start(bf16[8,2,2,32,1024]{4,3,2,1,0:T(8,128)(2,1)} %fusion.10), calls=%async_computation | async-start | bytes 4194304 | tf_op jit(solution)/shard_map/all_to_all | solution.py:117
  75.4 102.2 %copy-start.1 = (bf16[1,32,64]{2,1,0:T(8,128)(2,1)S(1)}, bf16[1,32,64]{2,1,0:T(8,128)(2,1)}, u32[]{:S(2)}) copy-start(bf16[1,32,64]{2,1,0:T(8,128)(2,1)} %param.21) | copy-start | bytes 12292
  75.5 106.6 %copy-start.2 = (f32[32,64]{1,0:T(8,128)S(1)}, f32[32,64]{1,0:T(8,128)}, u32[]{:S(2)}) copy-start(f32[32,64]{1,0:T(8,128)} %param.23) | copy-start | bytes 24580
Sparse Core Ops, SparseCore 0:
  9.5 11.7 all-gather.2
